TPU v7x, 512 devices: a whole 4x4x16 slice. The times are simulated.
512 devices in a mesh: gr: 2 (over z_hi), sp: 32 (over z_lo, y), tp: 8 (over x, core).
Axes of the slice: x: 4, y: 4, z: 16 (z_hi: 2, z_lo: 8; z = z_hi * 8 + z_lo), core: 2. Of those that a mesh axis runs over, the one named last changes fastest.
Arguments:
- tokens: bfloat16 [4, 32768, 2048], P('gr', ('sp', 'tp')), parts along dimension 0, may hold values from -6 to 6
- key_weight: bfloat16 [2048, 1024], P('sp'), may hold values from -0.125 to 0.125
- value_weight: bfloat16 [2048, 1024], P('sp'), may hold values from -0.125 to 0.125
- queries: bfloat16 [4, 1024], P('gr'), parts along dimension 0, may hold values from -6 to 6
- head_offset: float32 [16], replicated, may hold values from -14 to -3.5
- key_bias: bfloat16 [4, 32768, 16], P('gr', ('sp', 'tp')), parts along dimension 0, may hold values from -0.5 to 12.9
Outputs:
- key_cache: bfloat16 [4, 32768, 1024], P('gr', 'sp', 'tp'), parts along dimension 0
- value_cache: bfloat16 [4, 32768, 1024], P('gr', 'sp', 'tp'), parts along dimension 0
- bias_cache: bfloat16 [4, 32768, 16], P('gr', 'sp', 'tp'), parts along dimension 0
- reading: float32 [4, 1024], P('gr', 'tp'), parts along dimension 0
There are 2 independent parts, one for each index of `gr`. A program takes and returns all parts, laid end to end along the dimension named above; an argument that names none is the same for every part. Nothing has to cross between parts.
All inputs are finite; a program needn't handle non-finite values.
Results may differ from a plain program's by a relative error of at most 0.0052.
Values may be sent and summed in bfloat16 or wider, within the bound.
A program may use at most 64 MiB of HBM per device.

v0:
```python
import jax
import jax.numpy as jnp
from jax import lax
from jax.sharding import Mesh
from jax.sharding import PartitionSpec as P

TP = ("tp_0", "tp_1")
SP_TP = ("sp", "tp_0", "tp_1")


def joined_along(blocks, dim):
    dims = list(blocks.shape[1:])
    dims[dim] *= blocks.shape[0]
    return jnp.moveaxis(blocks, 0, dim).reshape(dims)


def copy_for_each(x, axis):
    copies = jnp.broadcast_to(x, (lax.axis_size(axis), *x.shape))
    return lax.all_to_all(copies, axis, split_axis=0, concat_axis=0, tiled=True)


def gathered_copies(x, axis, dim):
    return joined_along(copy_for_each(x, axis), dim)


def cut_along(x, dim, length):
    dims = x.shape
    blocks = x.reshape(*dims[:dim], length, dims[dim] // length, *dims[dim + 1 :])
    return jnp.moveaxis(blocks, dim, 0)


def exchange_in_order(blocks, axes, sequence):
    inside = blocks.shape[1:]
    result = blocks.reshape(*(lax.axis_size(a) for a in axes), *inside)
    for k in sequence:
        result = lax.all_to_all(result, axes[k], k, k, tiled=True)
    return result.reshape(-1, *inside)


def exchange_by_axis(x, axes, sequence, split_dim, concat_dim):
    blocks = cut_along(x, split_dim, lax.axis_size(axes))
    return joined_along(exchange_in_order(blocks, axes, sequence), concat_dim)


def folded_in_pairs(pieces, combine):
    while len(jax.tree.leaves(pieces)[0]) > 1:
        pieces = jax.vmap(combine)(*(pieces[side::2] for side in (0, 1)))
    return pieces[0]


def entering(x, axis, combine, identity):
    length, position = (lax.axis_size(axis), lax.axis_index(axis))
    passed = jnp.arange(length) > position

    def kept(part, zero, own):
        part = jnp.where(
            passed.reshape(-1, *(1 for _ in own.shape)), part, jnp.asarray(zero, own.dtype)
        )
        return part[::-1]

    pieces = copy_for_each(x, axis)
    return folded_in_pairs(kept(pieces, identity, x), combine)


def taken_together(x, axis):
    everything = copy_for_each(x, axis)
    return jnp.sum(everything, axis=0)


def add_terms(earlier, later):
    return earlier + later


def normalize(mixture):
    return mixture * lax.rsqrt(jnp.mean(mixture * mixture, axis=-1, keepdims=True) + 1e-06)


def per_device(tokens, key_weight, value_weight, queries, head_offset, key_bias):
    seq_count, pos_dev, model_width = tokens.shape
    head_count = head_offset.shape[0]
    kv_width = key_weight.shape[1]
    head_dim = kv_width // head_count
    score_scale = head_dim ** (-0.5)
    tp_count = lax.axis_size(TP)
    col_width = kv_width // tp_count
    col_start = lax.axis_index(TP) * col_width
    own_cols = jnp.concatenate(
        [
            lax.dynamic_slice_in_dim(key_weight, col_start, col_width, 1),
            lax.dynamic_slice_in_dim(value_weight, col_start, col_width, 1),
        ],
        axis=1,
    )
    full_cols = gathered_copies(own_cols, "sp", 0)
    projected = jnp.einsum(
        "spd,dw->spw",
        lax.all_gather(tokens, TP, axis=1, tiled=True),
        full_cols,
        preferred_element_type=jnp.float32,
    ).astype(jnp.bfloat16)
    key_cache = projected[:, :, :col_width]
    value_cache = projected[:, :, col_width:]
    bias_cache = exchange_by_axis(key_bias, TP, (1, 0), 2, 1)
    span_len = key_cache.shape[1]
    local_heads = bias_cache.shape[2]
    key_blocks = key_cache.reshape(seq_count, span_len, local_heads, head_dim)
    value_blocks = value_cache.reshape(seq_count, span_len, local_heads, head_dim)
    query_cols = lax.dynamic_slice_in_dim(queries, col_start, col_width, 1)
    query_heads = query_cols.reshape(seq_count, local_heads, head_dim)
    head_start = lax.axis_index(TP) * local_heads
    local_offset = lax.dynamic_slice_in_dim(head_offset, head_start, local_heads, 0)
    logits = (
        jnp.einsum("sphc,shc->shp", key_blocks, query_heads, preferred_element_type=jnp.float32)
        * score_scale
    )
    logits = (
        logits
        + local_offset[None, :, None]
        + jnp.transpose(bias_cache.astype(jnp.float32), (0, 2, 1))
    )
    fading = jax.nn.log_sigmoid(-logits)
    within = lax.cumsum(fading, axis=2, reverse=True) - fading
    block_total = jnp.sum(fading, axis=2)
    carried = entering(block_total, "sp", add_terms, jnp.zeros_like(block_total))
    weights = jnp.exp(jax.nn.log_sigmoid(logits) + within + carried[:, :, None]).astype(
        jnp.bfloat16
    )
    partial_value = jnp.einsum(
        "shp,sphc->shc", weights, value_blocks, preferred_element_type=jnp.float32
    )
    mixture = taken_together(partial_value, "sp")
    reading = normalize(mixture).reshape(seq_count, col_width)
    return (key_cache, value_cache, bias_cache, reading)


def solution(mesh):
    split = Mesh(
        mesh.devices.reshape(mesh.shape["gr"], mesh.shape["sp"], 4, 2), ("gr", "sp", "tp_0", "tp_1")
    )
    placed = (
        P("gr", SP_TP, None),
        P("sp", None),
        P("sp", None),
        P("gr", None),
        P(),
        P("gr", SP_TP, None),
    )
    return jax.shard_map(
        per_device,
        mesh=split,
        in_specs=placed,
        out_specs=(P("gr", "sp", TP), P("gr", "sp", TP), P("gr", "sp", TP), P("gr", TP)),
        check_vma=False,
    )
```

profile of v0, /device:TPU:1, one launch (start us, length us, event | category | flops | bytes accessed | tf_op | source)
XLA Modules:
  0.0 146.5 jit_solution(2500508803687826353)
XLA Ops:
  7.2 0.7 all-gather.2.cloned.1.call-update
  7.9 0.7 copy.37
  8.6 10.2 %all_to_all.25 = bf16[4,2,2,128,2]{3,0,4,2,1:T(4,128)(2,1)S(1)} all-to-all(bf16[4,2,2,128,2]{3,0,4,2,1:T(4,128)(2,1)S(1)} %copy.38), channel_id=1, replica_groups=mesh['gr'=2,'sp'=32,'tp_0'=4,'tp_1'=2] {'tp_1'}, dimensions={1} | all-to-all | bytes 16384 | tf_op jit(solution)/shard_map/all_to_all | solution.py:36
  18.8 0.6 copy.39
  19.4 3.2 %all-to-all-start.2 = ((bf16[4,2,2,128,2]{3,1,4,2,0:T(2,128)(2,1)}), bf16[4,2,2,128,2]{3,1,4,2,0:T(2,128)(2,1)S(1)}, u32[]{:S(2)}, u32[]{:S(2)}) async-start(bf16[4,2,2,128,2]{3,1,4,2,0:T(2,128)(2,1)} %copy.39), calls=%async_computation.2 | async-start | bytes 16384 | tf_op jit(solution)/shard_map/all_to_all | solution.py:36
  22.7 0.7 constant_dynamic-slice_fusion.1
  23.4 3.4 %all-to-all-done.2 = bf16[4,2,2,128,2]{3,1,4,2,0:T(2,128)(2,1)S(1)} async-done(((bf16[4,2,2,128,2]{3,1,4,2,0:T(2,128)(2,1)}), bf16[4,2,2,128,2]{3,1,4,2,0:T(2,128)(2,1)S(1)}, u32[]{:S(2)}, u32[]{:S(2)}) %all-to-all-start.2) | async-done | bytes 8224 | tf_op jit(solution)/shard_map/all_to_all | solution.py:36
  26.8 1.2 broadcast_in_dim.23
  28.0 10.7 %all-to-all-start = ((bf16[32,64,256]{2,1,0:T(8,128)(2,1)}), bf16[32,64,256]{2,1,0:T(8,128)(2,1)S(1)}, u32[]{:S(2)}, u32[]{:S(2)}) async-start(bf16[32,64,256]{2,1,0:T(8,128)(2,1)} %broadcast_in_dim.23), calls=%async_computation | async-start | bytes 2097152 | tf_op jit(solution)/shard_map/all_to_all | solution.py:19
  38.8 0.7 dynamic_slice.15
  39.6 48.9 %all-to-all-done = bf16[32,64,256]{2,1,0:T(8,128)(2,1)S(1)} async-done(((bf16[32,64,256]{2,1,0:T(8,128)(2,1)}), bf16[32,64,256]{2,1,0:T(8,128)(2,1)S(1)}, u32[]{:S(2)}, u32[]{:S(2)}) %all-to-all-start) | async-done | bytes 1048608 | tf_op jit(solution)/shard_map/all_to_all | solution.py:19
  88.5 5.8 %fusion = bf16[2,1024,256]{1,2,0:T(8,128)(2,1)S(1)} fusion(bf16[2048,256,1]{1,0,2:T(8,128)(2,1)S(1)} %bitcast.51, bf16[2,1024,2048]{2,1,0:T(8,128)(2,1)} %all-gather.2.cloned.1.call-done), kind=kOutput, calls=%fused_computation.1 | convolution fusion | flops 2148007936 | bytes 10485760 | tf_op jit(solution)/shard_map/spd,dw->spw/dot_general | solution.py:95
  94.7 5.0 %reduce-window.6 = f32[2,2,8,128]{3,2,1,0:T(8,128)S(1)} reduce-window(f32[2,2,8,128]{3,2,1,0:T(8,128)S(1)} %reshape.68, f32[]{:T(128)} %constant.35.clone.1), window={size=1x1x1x128 pad=0_0x0_0x0_0x0_127}, to_apply=%region_0.1 | reduce-window | flops 520192 | bytes 32772 | tf_op jit(solution)/shard_map/reduce-window
  100.3 0.6 broadcast_in_dim.25
  101.0 8.1 %all-to-all-start.3 = ((f32[32,2,2]{2,1,0:T(2,128)}), f32[32,2,2]{2,1,0:T(2,128)S(1)}, u32[]{:S(2)}, u32[]{:S(2)}) async-start(f32[32,2,2]{2,1,0:T(2,128)} %broadcast_in_dim.25), calls=%async_computation.3 | async-start | bytes 65536 | tf_op jit(solution)/shard_map/all_to_all | solution.py:19
  109.1 11.5 %all-to-all-done.3 = f32[32,2,2]{2,1,0:T(2,128)S(1)} async-done(((f32[32,2,2]{2,1,0:T(2,128)}), f32[32,2,2]{2,1,0:T(2,128)S(1)}, u32[]{:S(2)}, u32[]{:S(2)}) %all-to-all-start.3) | async-done | bytes 544 | tf_op jit(solution)/shard_map/all_to_all | solution.py:19
  121.2 0.7 reshape.79
  122.0 3.9 %all-to-all-start.4 = ((f32[32,1,256]{2,1,0:T(1,128)}), f32[32,1,256]{2,1,0:T(1,128)S(1)}, u32[]{:S(2)}, u32[]{:S(2)}) async-start(f32[32,1,256]{2,1,0:T(1,128)} %reshape.79), calls=%async_computation.4 | async-start | bytes 65536 | tf_op jit(solution)/shard_map/all_to_all | solution.py:19
  125.8 1.0 copy.42
  126.8 1.0 copy.43
  127.8 9.6 %all-to-all-done.4 = f32[32,1,256]{2,1,0:T(1,128)S(1)} async-done(((f32[32,1,256]{2,1,0:T(1,128)}), f32[32,1,256]{2,1,0:T(1,128)S(1)}, u32[]{:S(2)}, u32[]{:S(2)}) %all-to-all-start.4) | async-done | bytes 32800 | tf_op jit(solution)/shard_map/all_to_all | solution.py:19
  137.4 0.5 broadcast.36
  138.0 0.7 reduce.2
  139.0 0.7 mul.39
  (39 shorter events, 2.2 us)
Async XLA Ops:
  7.2 31.6 %copy-start = (bf16[2,1024]{1,0:T(2,128)(2,1)S(1)}, bf16[2,1024]{1,0:T(2,128)(2,1)}, u32[]{:S(2)}) copy-start(bf16[2,1024]{1,0:T(2,128)(2,1)} %param.9) | copy-start | bytes 12292
  7.2 81.3 %all-gather.2.cloned.1.call-start = ((), (), s32[]{:S(2)}) async-start(), calls=%async_computation.5 | async-start | bytes 9437184 | tf_op jit(solution)/shard_map/all_gather | solution.py:97
  19.4 7.4 %all-to-all-start.2 = ((bf16[4,2,2,128,2]{3,1,4,2,0:T(2,128)(2,1)}), bf16[4,2,2,128,2]{3,1,4,2,0:T(2,128)(2,1)S(1)}, u32[]{:S(2)}, u32[]{:S(2)}) async-start(bf16[4,2,2,128,2]{3,1,4,2,0:T(2,128)(2,1)} %copy.39), calls=%async_computation.2 | async-start | bytes 16384 | tf_op jit(solution)/shard_map/all_to_all | solution.py:36
  28.0 60.5 %all-to-all-start = ((bf16[32,64,256]{2,1,0:T(8,128)(2,1)}), bf16[32,64,256]{2,1,0:T(8,128)(2,1)S(1)}, u32[]{:S(2)}, u32[]{:S(2)}) async-start(bf16[32,64,256]{2,1,0:T(8,128)(2,1)} %broadcast_in_dim.23), calls=%async_computation | async-start | bytes 2097152 | tf_op jit(solution)/shard_map/all_to_all | solution.py:19
  39.6 81.2 %copy-start.1 = (bf16[2,1024,2]{1,2,0:T(2,128)(2,1)}, bf16[2,1024,2]{1,2,0:T(2,128)(2,1)S(1)}, u32[]{:S(2)}) copy-start(bf16[2,1024,2]{1,2,0:T(2,128)(2,1)S(1)} %reshape.65) | copy-start | bytes 24580
  101.0 19.7 %all-to-all-start.3 = ((f32[32,2,2]{2,1,0:T(2,128)}), f32[32,2,2]{2,1,0:T(2,128)S(1)}, u32[]{:S(2)}, u32[]{:S(2)}) async-start(f32[32,2,2]{2,1,0:T(2,128)} %broadcast_in_dim.25), calls=%async_computation.3 | async-start | bytes 65536 | tf_op jit(solution)/shard_map/all_to_all | solution.py:19
  122.0 15.5 %all-to-all-start.4 = ((f32[32,1,256]{2,1,0:T(1,128)}), f32[32,1,256]{2,1,0:T(1,128)S(1)}, u32[]{:S(2)}, u32[]{:S(2)}) async-start(f32[32,1,256]{2,1,0:T(1,128)} %reshape.79), calls=%async_computation.4 | async-start | bytes 65536 | tf_op jit(solution)/shard_map/all_to_all | solution.py:19
Sparse Core Ops, SparseCore 0:
  10.1 62.9 all-gather.1
where the time goes:
time: 148 us; the launch traced here: 147 us
  waiting for transfers between devices  74.1 us (50%)
  starting transfers between devices  25.9 us (18%)
  between operations  14.2 us (10%)
  blocking collectives  10.2 us (7%)
  local copies, waits for them, and re-layouts  9.02 us (6%)
  other arithmetic  6.85 us (5%)
  matrix products  6.23 us (4%)
    all_to_all x3, waiting for transfers between devices, copy_for_each(): return lax.all_to_all(copies, axis, split_axis=0, concat_axis=0, tiled=True)  70 us
    all_to_all x3, starting transfers between devices, copy_for_each(): return lax.all_to_all(copies, axis, split_axis=0, concat_axis=0, tiled=True)  22.6 us
    all_to_all x1, blocking collectives, exchange_in_order(): result = lax.all_to_all(result, axes[k], k, k, tiled=True)  10.2 us
    dot_general x1, matrix products, per_device(): jnp.einsum('spd,dw->spw', lax.all_gather(tokens, TP, axis=1, tiled=True),...  5.81 us
    another operation x2, other arithmetic  5.33 us
    all_to_all x1, waiting for transfers between devices, exchange_in_order(): result = lax.all_to_all(result, axes[k], k, k, tiled=True)  3.37 us
    all_to_all x1, starting transfers between devices, exchange_in_order(): result = lax.all_to_all(result, axes[k], k, k, tiled=True)  3.25 us
  transfers between devices with their start and end apart: 5, of which 4 were waited for; matrix products, arithmetic and copies ran while one was open for 4% of the time, Pallas kernels for 0%

commit v1 on v0

v1 whole, which is shorter than its diff:
```python
import functools

import jax
import jax.numpy as jnp
from jax import lax
from jax.experimental import pallas as pl
from jax.experimental.pallas import tpu as pltpu
from jax.sharding import PartitionSpec as P

MESH = pl.DeviceIdType.MESH
CHUNKS = 8
EARLY = 4


def strictly_later(size):
    row = lax.broadcasted_iota(jnp.int32, (size, size), 0)
    col = lax.broadcasted_iota(jnp.int32, (size, size), 1)
    return jnp.where(row > col, 1.0, 0.0).astype(jnp.float32)


def kernel(
    tok_ref, kw_ref, vw_ref, q_ref, off_ref, bias_ref,
    key_out, value_out, bias_out, read_out,
    tbuf, wa, wb, kv, bb, bsel, part, r1, mid, r2, rd,
    load_sem, t_send, t_recv, s_send, s_recv, b_send, b_recv,
    ay_send, ay_recv, az_send, az_recv, bz_send, bz_recv, by_send, by_recv,
    o_send, o_recv, st_sem, f1_send, f1_recv, f2_send, f2_recv, hello,
):
    gr, sp, tp = lax.axis_index("gr"), lax.axis_index("sp"), lax.axis_index("tp")
    zl, y = sp // 4, sp % 4
    z = gr * 8 + zl
    x, c = tp // 2, tp % 2
    px, ox = x + 1 - 2 * (x % 2), 3 - x
    half = x // 2
    ptp, otp, stp = px * 2 + c, ox * 2 + c, x * 2 + 1 - c
    dm = (x % 2) * 2 + c
    ds = (x % 2) * 2 + 1 - c
    dp = (1 - x % 2) * 2 + c
    dq = (1 - x % 2) * 2 + 1 - c

    def at_tp(t):
        return (gr, sp, t)

    def at_y(k):
        return (gr, zl * 4 + (y + k) % 4, tp)

    def at_z(k):
        there = (z + k + 16) % 16
        return (there // 8, (there % 8) * 4 + y, tp)

    def remote(src, dst, send, recv, device):
        return pltpu.make_async_remote_copy(
            src_ref=src, dst_ref=dst, send_sem=send, recv_sem=recv,
            device_id=device, device_id_type=MESH,
        )

    pending = []

    def push(*args):
        copy = remote(*args)
        copy.start()
        pending.append(copy)

    tok_load = pltpu.make_async_copy(tok_ref, tbuf.at[dm], load_sem.at[0])
    tok_load.start()
    own_rows = pl.ds(pl.multiple_of(sp * 64, 64), 64)
    loads = []
    for n, (w_ref, lane) in enumerate(((kw_ref, 0), (vw_ref, 128))):
        for m, (buf, t) in enumerate(((wa, tp), (wb, otp))):
            cols = pl.ds(pl.multiple_of(t * 128, 128), 128)
            load = pltpu.make_async_copy(
                w_ref.at[:, cols], buf.at[own_rows, pl.ds(lane, 128)],
                load_sem.at[1 + n * 2 + m],
            )
            load.start()
            loads.append(load)
    bias_load = pltpu.make_async_copy(bias_ref, bb.at[tp], load_sem.at[5])
    bias_load.start()

    barrier = pltpu.get_barrier_semaphore()
    greeted = [at_tp((tp + k) % 8) for k in range(1, 8)]
    greeted += [at_y(k) for k in range(1, 4)]
    greeted += [(gr, zl * 4 + (y + k) % 4, otp) for k in range(1, 4)]
    greeted += [at_z(1), at_z(-1)]
    for device in greeted:
        pl.semaphore_signal(barrier, inc=1, device_id=device, device_id_type=MESH)
    pl.semaphore_wait(barrier, len(greeted))

    rows_of = 256 // CHUNKS

    def t_copy(k):
        piece = (dm, pl.ds(k * rows_of, rows_of))
        return remote(tbuf.at[piece], tbuf.at[piece], t_send.at[k], t_recv.at[k], at_tp(ptp))

    def t_arrival(k):
        piece = (dp, pl.ds(k * rows_of, rows_of))
        return remote(tbuf.at[piece], tbuf.at[piece], t_send.at[k], t_recv.at[k], at_tp(ptp))

    def t_forward(k):
        piece = (dp, pl.ds(k * rows_of, rows_of))
        return remote(tbuf.at[piece], tbuf.at[piece], s_send.at[k], s_recv.at[k], at_tp(stp))

    def s_arrival(k):
        piece = (dq, pl.ds(k * rows_of, rows_of))
        return remote(tbuf.at[piece], tbuf.at[piece], s_send.at[k], s_recv.at[k], at_tp(stp))

    for load in loads:
        load.wait()
    for k in range(1, 4):
        push(wa.at[own_rows], wa.at[own_rows], ay_send.at[k - 1], ay_recv.at[k - 1], at_y(k))

    def b_rows(offset, start=0, size=64):
        block = (zl + offset + 8) % 8
        return pl.ds(pl.multiple_of(block * 256 + y * 64 + start, 32), size)

    def b_rows_from(k, offset):
        block = (zl + offset + 8) % 8
        return pl.ds(pl.multiple_of(block * 256 + ((y - k + 4) % 4) * 64, 64), 64)

    def a_rows(offset, start=0, size=256):
        block = (zl + offset + 8) % 8
        return pl.ds(pl.multiple_of(block * 256 + start, 128), size)

    def b_spread(q, offset):
        for k in range(1, 4):
            n = q * 3 + k - 1
            push(wb.at[b_rows(offset)], wb.at[b_rows(offset)], by_send.at[n], by_recv.at[n], at_y(k))

    def b_z(side, j):
        sign = 1 if side == 0 else -1
        if j < 4:
            rows = b_rows(-sign * (j - 1))
        else:
            rows = b_rows(-sign * 3, 32 * side, 32)
        n = side * 4 + j - 1
        push(wb.at[rows], wb.at[rows], bz_send.at[n], bz_recv.at[n], at_z(sign))

    def b_z_wait(side, j):
        sign = 1 if side == 0 else -1
        rows = b_rows(-sign * j) if j < 4 else b_rows(4, 32 * side, 32)
        n = side * 4 + j - 1
        remote(wb.at[rows], wb.at[rows], bz_send.at[n], bz_recv.at[n], at_z(sign)).wait_recv()

    def a_z(side, j):
        sign = 1 if side == 0 else -1
        if j < 4:
            rows = a_rows(-sign * (j - 1))
        else:
            rows = a_rows(-sign * 3, 128 * side, 128)
        n = side * 4 + j - 1
        push(wa.at[rows], wa.at[rows], az_send.at[n], az_recv.at[n], at_z(sign))

    def a_z_wait(side, j):
        sign = 1 if side == 0 else -1
        rows = a_rows(-sign * j) if j < 4 else a_rows(4, 128 * side, 128)
        n = side * 4 + j - 1
        remote(wa.at[rows], wa.at[rows], az_send.at[n], az_recv.at[n], at_z(sign)).wait_recv()

    b_z(0, 1)
    b_z(1, 1)
    tok_load.wait()
    for k in range(CHUNKS):
        copy = t_copy(k)
        copy.start()
        pending.append(copy)
    push(tbuf.at[dm], tbuf.at[dm], s_send.at[CHUNKS], s_recv.at[CHUNKS], at_tp(stp))
    b_spread(0, 0)
    bias_load.wait()
    for k in range(1, 8):
        push(bb.at[tp], bb.at[tp], b_send.at[k - 1], b_recv.at[k - 1], at_tp((tp + k) % 8))

    for k in range(1, 4):
        rows = pl.ds(pl.multiple_of(zl * 256 + ((y - k + 4) % 4) * 64, 64), 64)
        remote(wa.at[rows], wa.at[rows], ay_send.at[k - 1], ay_recv.at[k - 1], at_y(k)).wait_recv()
    a_z(0, 1)
    a_z(1, 1)

    def b_step(j):
        for side in (0, 1):
            b_z_wait(side, j)
            if j < 4:
                b_z(side, j + 1)
                b_spread(2 * j - 1 + side, -j if side == 0 else j)
        if j == 4:
            b_spread(7, 4)

    def a_step(j):
        for side in (0, 1):
            a_z_wait(side, j)
            if j < 4:
                a_z(side, j + 1)

    def forward_step(k):
        t_arrival(k).wait_recv()
        copy = t_forward(k)
        copy.start()
        pending.append(copy)

    b_step(1)
    b_step(2)
    a_step(1)
    forward_step(0)
    b_step(3)
    a_step(2)
    forward_step(1)
    b_step(4)
    a_step(3)
    forward_step(2)
    a_step(4)
    forward_step(3)
    offsets = (0, -1, 1, -2, 2, -3, 3, 4)
    for q in range(8):
        for k in range(1, 4):
            n = q * 3 + k - 1
            rows = b_rows_from(k, offsets[q])
            remote(wb.at[rows], wb.at[rows], by_send.at[n], by_recv.at[n], at_y(k)).wait_recv()

    def project(tokens, s, d, first, count):
        for g, w in enumerate((wa, wb)):
            out = jnp.dot(tokens, w[...], preferred_element_type=jnp.float32).astype(jnp.bfloat16)
            for n in range(len(d)):
                rows = out[n * count : (n + 1) * count]
                kv[g, 0, s, d[n], pl.ds(first, count), :] = rows[:, :128]
                kv[g, 1, s, d[n], pl.ds(first, count), :] = rows[:, 128:]

    outs = (key_out, value_out)

    def o_copy(s, d, v, where):
        n = d * 4 + s * 2 + v
        return remote(
            kv.at[1, v, s, d], outs[v].at[s, where, d], o_send.at[n], o_recv.at[n], at_tp(otp)
        )

    def send_out(s, d):
        for v in (0, 1):
            o_copy(s, d, v, half).start()

    remote(tbuf.at[ds], tbuf.at[ds], s_send.at[CHUNKS], s_recv.at[CHUNKS], at_tp(stp)).wait_recv()

    def early(n, carry):
        s, which = n % 2, n // 2
        d = jnp.where(which == 0, dm, ds)
        project(tbuf[d, pl.ds(pl.multiple_of(s * 128, 128), 128), :], s, (d,), 0, 128)
        send_out(s, d)
        return carry

    lax.fori_loop(0, 4, early, 0)
    for k in range(EARLY):
        s_arrival(k).wait_recv()

    def early_partner(n, carry):
        d = jnp.where(n == 0, dp, dq)
        project(tbuf[d, pl.ds(0, 128), :], 0, (d,), 0, 128)
        send_out(0, d)
        return carry

    lax.fori_loop(0, 2, early_partner, 0)

    def up():
        @pl.when(zl > 0)
        def _():
            pl.semaphore_wait(hello.at[0], 1)

        @pl.when(zl < 7)
        def _():
            pl.semaphore_signal(hello.at[0], inc=1, device_id=at_z(1), device_id_type=MESH)

    def down():
        @pl.when(zl < 7)
        def _():
            pl.semaphore_wait(hello.at[1], 1)

        @pl.when(zl > 0)
        def _():
            pl.semaphore_signal(hello.at[1], inc=1, device_id=at_z(-1), device_id_type=MESH)

    @pl.when(zl < 4)
    def _():
        up()
        down()

    @pl.when(zl >= 4)
    def _():
        down()
        up()

    def late(k, carry):
        t_arrival(k).wait_recv()
        t_forward(k).start()
        s_arrival(k).wait_recv()
        first = pl.multiple_of((k - EARLY) * rows_of, rows_of)
        here = pl.ds(pl.multiple_of(k * rows_of, rows_of), rows_of)
        both = jnp.concatenate([tbuf[dp, here, :], tbuf[dq, here, :]], axis=0)
        project(both, 1, (dp, dq), first, rows_of)
        return carry

    lax.fori_loop(EARLY, CHUNKS, late, 0)
    send_out(1, dp)
    send_out(1, dq)

    stores = []
    for v in (0, 1):
        for s in (0, 1):
            store = pltpu.make_async_copy(kv.at[0, v, s], outs[v].at[s, half], st_sem.at[v * 2 + s])
            store.start()
            stores.append(store)

    for k in range(1, 8):
        src = (tp - k + 8) % 8
        remote(bb.at[src], bb.at[src], b_send.at[k - 1], b_recv.at[k - 1], at_tp(src)).wait_recv()
    row = lax.broadcasted_iota(jnp.int32, (8, 32), 0)
    col = lax.broadcasted_iota(jnp.int32, (8, 32), 1)
    group_tp = jnp.where(row < 4, tp, otp)
    wanted = ((row // 2) % 2) * 16 + group_tp * 2 + row % 2
    select = jnp.where(col == wanted, 1.0, 0.0).astype(jnp.bfloat16)
    for d in range(8):
        picked = jnp.dot(select, bb[d].reshape(32, 128), preferred_element_type=jnp.float32)
        bsel[d] = picked
        for s in (0, 1):
            bias_out_rows = picked[2 * s : 2 * s + 2].astype(jnp.bfloat16)
            rd_rows = pl.ds(d * 128, 128)
            part_bias(bias_out, s, rd_rows, bias_out_rows)

    lane = lax.broadcasted_iota(jnp.int32, (8, 128), 1)
    row8 = lax.broadcasted_iota(jnp.int32, (8, 128), 0)
    own_lane = (lane // 64) == (row8 % 2)
    hrow = lax.broadcasted_iota(jnp.int32, (8, 16), 0)
    hcol = lax.broadcasted_iota(jnp.int32, (8, 16), 1)
    head = jnp.where(hrow < 4, tp, otp) * 2 + hrow % 2
    offset = jnp.sum(
        jnp.where(hcol == head, jnp.broadcast_to(off_ref[...], (8, 16)), 0.0), axis=1, keepdims=True
    )
    queries = []
    for g, t in enumerate((tp, otp)):
        cols = q_ref[:, pl.ds(pl.multiple_of(t * 128, 128), 128)].astype(jnp.float32)
        for s in (0, 1):
            mine = own_lane & (row8 // 2 == g * 2 + s)
            spread = jnp.broadcast_to(cols[s : s + 1], (8, 128))
            queries.append(jnp.where(mine, spread, 0.0).astype(jnp.bfloat16))
    later = strictly_later(128)
    ls, within, totals = [], [], []
    for d in range(4):
        score = jnp.zeros((8, 128), jnp.float32)
        for g in (0, 1):
            for s in (0, 1):
                score += lax.dot_general(
                    queries[g * 2 + s], kv[g, 0, s, d], (((1,), (1,)), ((), ())),
                    preferred_element_type=jnp.float32,
                )
        logit = score * 0.125 + offset + bsel[half * 4 + d]
        tail = jnp.log1p(jnp.exp(-jnp.abs(logit)))
        fading = -(jnp.maximum(logit, 0.0) + tail)
        ls.append(jnp.minimum(logit, 0.0) - tail)
        within.append(
            jnp.dot(fading, later, precision=lax.Precision.HIGHEST, preferred_element_type=jnp.float32)
        )
        totals.append(jnp.sum(fading, axis=1, keepdims=True))
    carried = jnp.zeros((8, 1), jnp.float32)
    mixture = jnp.zeros((8, 128), jnp.float32)
    for d in (3, 2, 1, 0):
        weight = jnp.exp(ls[d] + within[d] + carried)
        carried = carried + totals[d]
        high = weight.astype(jnp.bfloat16)
        low = (weight - high.astype(jnp.float32)).astype(jnp.bfloat16)
        for g in (0, 1):
            for s in (0, 1):
                values = kv[g, 1, s, d]
                product = jnp.dot(high, values, preferred_element_type=jnp.float32)
                product += jnp.dot(low, values, preferred_element_type=jnp.float32)
                mixture += jnp.where(row8 // 2 == g * 2 + s, product, 0.0)
    mixture = jnp.where(own_lane, mixture, 0.0)
    sums = jnp.where(own_lane, jnp.broadcast_to(carried, (8, 128)), 0.0)
    for g in (0, 1):
        lines = []
        for block in (mixture, sums):
            for s in (0, 1):
                r = g * 4 + s * 2
                lines.append(block[r : r + 1] + block[r + 1 : r + 2])
        part[g] = jnp.concatenate(lines, axis=0)

    def f1(slot, device, g):
        return remote(part.at[g], r1.at[slot], f1_send.at[g * 4 + slot // 2], f1_recv.at[slot], device)

    mine = y * 2 + half
    firsts = []
    for k in range(1, 4):
        copy = remote(part.at[0], r1.at[mine], f1_send.at[k], f1_recv.at[mine], at_y(k))
        copy.start()
        firsts.append(copy)
    for k in range(0, 4):
        device = (gr, zl * 4 + (y + k) % 4, otp)
        copy = remote(part.at[1], r1.at[mine], f1_send.at[4 + k], f1_recv.at[mine], device)
        copy.start()
        firsts.append(copy)
    own = pltpu.make_async_copy(part.at[0], r1.at[mine], f1_send.at[0])
    own.start()
    own.wait()
    for k in range(1, 4):
        slot = ((y + k) % 4) * 2 + half
        remote(part.at[0], r1.at[slot], f1_send.at[k], f1_recv.at[slot], at_y(k)).wait_recv()
    for k in range(0, 4):
        slot = ((y + k) % 4) * 2 + 1 - half
        remote(part.at[1], r1.at[slot], f1_send.at[4 + k], f1_recv.at[slot], at_tp(otp)).wait_recv()

    def combine(buf):
        total = buf[7][2:4]
        mixed = buf[7][0:2]
        for n in range(6, -1, -1):
            block = buf[n]
            mixed = mixed + block[0:2] * jnp.exp(total)
            total = total + block[2:4]
        return mixed, total

    mixed, total = combine(r1)
    mid[...] = jnp.concatenate([mixed, total], axis=0)
    seconds = []
    for k in range(1, 8):
        device = (gr, ((zl + k) % 8) * 4 + y, tp)
        copy = remote(mid, r2.at[zl], f2_send.at[k], f2_recv.at[zl], device)
        copy.start()
        seconds.append(copy)
    own = pltpu.make_async_copy(mid, r2.at[zl], f2_send.at[0])
    own.start()
    own.wait()
    for k in range(1, 8):
        slot = (zl + k) % 8
        remote(mid, r2.at[slot], f2_send.at[k], f2_recv.at[slot], at_z(1)).wait_recv()
    mixed, total = combine(r2)
    square = mixed * mixed
    first_head = lax.broadcasted_iota(jnp.int32, (2, 128), 1) < 64
    mean_a = jnp.sum(jnp.where(first_head, square, 0.0), axis=1, keepdims=True) * (1.0 / 64)
    mean_b = jnp.sum(jnp.where(first_head, 0.0, square), axis=1, keepdims=True) * (1.0 / 64)
    read_out[...] = mixed * lax.rsqrt(jnp.where(first_head, mean_a, mean_b) + 1e-06)

    for copy in pending + firsts + seconds:
        copy.wait_send()

    def forwarded(k, carry):
        t_forward(k).wait_send()
        return carry

    lax.fori_loop(EARLY, CHUNKS, forwarded, 0)

    def sent(n, carry):
        s, d = n % 2, n // 2
        for v in (0, 1):
            copy = o_copy(s, d, v, half)
            copy.wait_send()
            o_copy(s, d, v, 1 - half).wait_recv()
        return carry

    lax.fori_loop(0, 8, sent, 0)
    for store in stores:
        store.wait()


def part_bias(bias_out, s, cols, rows):
    bias_out[s, :, cols] = rows


def per_device(tokens, key_weight, value_weight, queries, head_offset, key_bias):
    any_space = pl.BlockSpec(memory_space=pl.ANY)
    vmem = pl.BlockSpec(memory_space=pltpu.VMEM)
    dma = pltpu.SemaphoreType.DMA
    cache = jax.ShapeDtypeStruct((2, 2, 4, 128, 128), jnp.bfloat16)
    keys, values, bias, reading = pl.pallas_call(
        kernel,
        out_shape=(
            cache,
            cache,
            jax.ShapeDtypeStruct((2, 2, 1024), jnp.bfloat16),
            jax.ShapeDtypeStruct((2, 128), jnp.float32),
        ),
        in_specs=[any_space, any_space, any_space, vmem, vmem, any_space],
        out_specs=(any_space, any_space, vmem, vmem),
        scratch_shapes=[
            pltpu.VMEM((4, 256, 2048), jnp.bfloat16),
            pltpu.VMEM((2048, 256), jnp.bfloat16),
            pltpu.VMEM((2048, 256), jnp.bfloat16),
            pltpu.VMEM((2, 2, 2, 4, 128, 128), jnp.bfloat16),
            pltpu.VMEM((8, 2, 16, 128), jnp.bfloat16),
            pltpu.VMEM((8, 8, 128), jnp.float32),
            pltpu.VMEM((2, 4, 128), jnp.float32),
            pltpu.VMEM((8, 4, 128), jnp.float32),
            pltpu.VMEM((4, 128), jnp.float32),
            pltpu.VMEM((8, 4, 128), jnp.float32),
            pltpu.VMEM((2, 128), jnp.float32),
            dma((6,)),
            dma((CHUNKS,)), dma((CHUNKS,)), dma((CHUNKS + 1,)), dma((CHUNKS + 1,)),
            dma((7,)), dma((7,)),
            dma((3,)), dma((3,)), dma((8,)), dma((8,)), dma((8,)), dma((8,)),
            dma((24,)), dma((24,)),
            dma((16,)), dma((16,)), dma((4,)),
            dma((8,)), dma((8,)), dma((8,)), dma((8,)),
            pltpu.SemaphoreType.REGULAR((2,)),
        ],
        name="prefill",
        compiler_params=pltpu.CompilerParams(collective_id=0, has_side_effects=True),
    )(
        tokens.reshape(256, 2048),
        key_weight,
        value_weight,
        queries,
        head_offset.reshape(1, 16),
        jnp.transpose(key_bias, (0, 2, 1)),
    )
    return (
        keys.reshape(2, 1024, 128),
        values.reshape(2, 1024, 128),
        jnp.transpose(bias, (0, 2, 1)),
        reading,
    )


def solution(mesh):
    placed = (
        P("gr", ("sp", "tp"), None),
        P("sp", None),
        P("sp", None),
        P("gr", None),
        P(),
        P("gr", ("sp", "tp"), None),
    )
    return jax.shard_map(
        per_device,
        mesh=mesh,
        in_specs=placed,
        out_specs=(P("gr", "sp", "tp"), P("gr", "sp", "tp"), P("gr", "sp", "tp"), P("gr", "tp")),
        check_vma=False,
    )
```

time: 148 us -> 72.6 us (0.49)
  the two profiles are of different devices: /device:TPU:1 before, /device:TPU:6 now
where the time goes in v1:
time: 72.6 us; the launch traced here: 72.4 us
  Pallas kernels  67.8 us (93%)
  local copies, waits for them, and re-layouts  3.95 us (5%)
    pallas_call x1, Pallas kernels, per_device(): pl.pallas_call(kernel, out_shape=(cache, cache, jax.ShapeDtypeStruct((2,...  67.8 us
    unnamed x10, local copies, waits for them, and re-layouts  3.95 us

profile of v1, /device:TPU:6, one launch (start us, length us, event | category | flops | bytes accessed | tf_op | source)
XLA Modules:
  0.0 72.4 jit_solution(15474064158108014683)
XLA Ops:
  0.6 67.8 %prefill.1 = (bf16[2,2,4,128,128]{4,3,2,1,0:T(8,128)(2,1)}, bf16[2,2,4,128,128]{4,3,2,1,0:T(8,128)(2,1)}, bf16[2,2,1024]{2,1,0:T(2,128)(2,1)}, f32[2,128]{1,0:T(2,128)}) custom-call(bf16[256,2048]{1,0:T(8,128)(2,1)} %bitcast.6, bf16[64,1024]{1,0:T(8,128)(2,1)} %kw_ref.1, bf16[64,1024]{1,0:T(8,128)(2,1)} %vw_ref.1, bf16[2,1024]{1,0:T(2,128)(2,1)} %q_ref.1, ...), custom_call_target="tpu_custom_call" | custom-call | tf_op jit(solution)/shard_map/prefill/pallas_call | solution.py:466
  68.5 0.0 copy-start
  68.5 1.9 %copy.14 = bf16[2,1024,128]{2,1,0:T(8,128)(2,1)} copy(bf16[2,1024,128]{2,1,0:T(8,128)(2,1)} %bitcast.8) | data formatting | bytes 1048576
  70.4 0.0 copy-done
  70.4 0.0 copy-start.1
  70.4 0.8 %copy.15 = bf16[2,1024,128]{2,1,0:T(8,128)(2,1)} copy(bf16[2,1024,128]{2,1,0:T(8,128)(2,1)S(1)} %bitcast.7) | data formatting | bytes 1048576
  71.2 0.0 copy-done.1
  71.2 0.0 copy-start.2
  71.2 0.6 copy.16
  71.8 0.1 copy-done.2
  71.9 0.6 copy.17
Async XLA Ops:
  68.5 1.9 %copy-start = (bf16[2,2,4,128,128]{4,3,2,1,0:T(8,128)(2,1)S(1)}, bf16[2,2,4,128,128]{4,3,2,1,0:T(8,128)(2,1)}, u32[]{:S(2)}) copy-start(bf16[2,2,4,128,128]{4,3,2,1,0:T(8,128)(2,1)} %get-tuple-element.9) | copy-start | bytes 1572868
  70.4 0.8 %copy-start.1 = (bf16[2,2,1024]{2,1,0:T(2,128)(2,1)S(1)}, bf16[2,2,1024]{2,1,0:T(2,128)(2,1)}, u32[]{:S(2)}) copy-start(bf16[2,2,1024]{2,1,0:T(2,128)(2,1)} %get-tuple-element.10) | copy-start | bytes 24580
  71.2 0.7 copy-start.2

commit v2 on v1

v2 whole, which is shorter than its diff:
```python
import functools

import jax
import jax.numpy as jnp
from jax import lax
from jax.experimental import pallas as pl
from jax.experimental.pallas import tpu as pltpu
from jax.sharding import PartitionSpec as P

MESH = pl.DeviceIdType.MESH
CHUNKS = 8
EARLY = 4


def strictly_later(size):
    row = lax.broadcasted_iota(jnp.int32, (size, size), 0)
    col = lax.broadcasted_iota(jnp.int32, (size, size), 1)
    return jnp.where(row > col, 1.0, 0.0).astype(jnp.float32)


def kernel(
    tok_ref, kw_ref, vw_ref, q_hbm, off_hbm, bias_ref,
    cache_out, bias_out, read_out,
    tbuf, wa, wb, kv, bb, bsel, part, r1, mid, r2, q_ref, off_ref,
    load_sem, t_send, t_recv, s_send, s_recv, b_send, b_recv,
    ay_send, ay_recv, z_send, z_recv, by_send, by_recv,
    o_send, o_recv, f1_send, f1_recv, f2_send, f2_recv, hello,
):
    gr, sp, tp = lax.axis_index("gr"), lax.axis_index("sp"), lax.axis_index("tp")
    zl, y = sp // 4, sp % 4
    z = gr * 8 + zl
    x, c = tp // 2, tp % 2
    px, ox = x + 1 - 2 * (x % 2), 3 - x
    half = x // 2
    ptp, otp, stp = px * 2 + c, ox * 2 + c, x * 2 + 1 - c
    dm = (x % 2) * 2 + c
    ds = (x % 2) * 2 + 1 - c
    dp = (1 - x % 2) * 2 + c
    dq = (1 - x % 2) * 2 + 1 - c

    def at_tp(t):
        return (gr, sp, t)

    def at_y(k):
        return (gr, zl * 4 + (y + k) % 4, tp)

    def at_z(k):
        there = (z + k + 16) % 16
        return (there // 8, (there % 8) * 4 + y, tp)

    def remote(src, dst, send, recv, device):
        return pltpu.make_async_remote_copy(
            src_ref=src, dst_ref=dst, send_sem=send, recv_sem=recv,
            device_id=device, device_id_type=MESH,
        )

    pending = []

    def push(*args):
        copy = remote(*args)
        copy.start()
        pending.append(copy)

    tok_load = pltpu.make_async_copy(tok_ref, tbuf.at[dm], load_sem.at[0])
    tok_load.start()
    own_rows = pl.ds(pl.multiple_of(sp * 64, 64), 64)
    loads = []
    for n, (w_ref, lane) in enumerate(((kw_ref, 0), (vw_ref, 128))):
        for m, (buf, t) in enumerate(((wa, tp), (wb, otp))):
            cols = pl.ds(pl.multiple_of(t * 128, 128), 128)
            load = pltpu.make_async_copy(
                w_ref.at[:, cols], buf.at[own_rows, pl.ds(lane, 128)],
                load_sem.at[1 + n * 2 + m],
            )
            load.start()
            loads.append(load)
    bias_load = pltpu.make_async_copy(bias_ref, bb.at[tp], load_sem.at[5])
    bias_load.start()
    q_load = pltpu.make_async_copy(q_hbm, q_ref, load_sem.at[6])
    q_load.start()
    off_load = pltpu.make_async_copy(off_hbm, off_ref, load_sem.at[7])
    off_load.start()

    barrier = pltpu.get_barrier_semaphore()
    lowest, highest = z == 0, z == 15

    def greet(device):
        pl.semaphore_signal(barrier, inc=1, device_id=device, device_id_type=MESH)

    for k in (2, 1, 3):
        greet(at_y(k))
    for k in range(1, 8):
        greet(at_tp((tp + k) % 8))

    @pl.when(jnp.logical_not(highest))
    def _():
        greet(at_z(1))

    @pl.when(jnp.logical_not(lowest))
    def _():
        greet(at_z(-1))
        pl.semaphore_wait(barrier, 12)

    @pl.when(lowest)
    def _():
        pl.semaphore_wait(barrier, 11)
        greet(at_z(-1))

    @pl.when(highest)
    def _():
        greet(at_z(1))

    rows_of = 256 // CHUNKS

    def t_copy(k):
        piece = (dm, pl.ds(k * rows_of, rows_of))
        return remote(tbuf.at[piece], tbuf.at[piece], t_send.at[k], t_recv.at[k], at_tp(ptp))

    def t_arrival(k):
        piece = (dp, pl.ds(k * rows_of, rows_of))
        return remote(tbuf.at[piece], tbuf.at[piece], t_send.at[k], t_recv.at[k], at_tp(ptp))

    def t_forward(k):
        piece = (dp, pl.ds(k * rows_of, rows_of))
        return remote(tbuf.at[piece], tbuf.at[piece], s_send.at[k], s_recv.at[k], at_tp(stp))

    def s_arrival(k):
        piece = (dq, pl.ds(k * rows_of, rows_of))
        return remote(tbuf.at[piece], tbuf.at[piece], s_send.at[k], s_recv.at[k], at_tp(stp))

    def forward_step(k):
        t_arrival(k).wait_recv()
        copy = t_forward(k)
        copy.start()
        pending.append(copy)

    tok_load.wait()
    for k in range(CHUNKS):
        copy = t_copy(k)
        copy.start()
        pending.append(copy)
    push(tbuf.at[dm], tbuf.at[dm], s_send.at[CHUNKS], s_recv.at[CHUNKS], at_tp(stp))

    shifts = (0, 0, 1, 3, 2)

    def rows_at(offset, shift, start=0, size=64):
        block = (zl + offset + 8) % 8
        return pl.ds(pl.multiple_of(block * 256 + ((y - shift + 4) % 4) * 64 + start, 32), size)

    def z_piece(p, offset, start=0, size=64):
        return (wb if p == 0 else wa).at[rows_at(offset, shifts[p], start, size)]

    def z_push(side, p, j):
        sign = 1 if side == 0 else -1
        if j < 4:
            piece = z_piece(p, -sign * (j - 1))
        else:
            piece = z_piece(p, -sign * 3, 32 * side, 32)
        n = (side * 5 + p) * 4 + j - 1
        push(piece, piece, z_send.at[n], z_recv.at[n], at_z(sign))

    def z_wait(side, p, j):
        sign = 1 if side == 0 else -1
        piece = z_piece(p, -sign * j) if j < 4 else z_piece(p, 4, 32 * side, 32)
        n = (side * 5 + p) * 4 + j - 1
        remote(piece, piece, z_send.at[n], z_recv.at[n], at_z(sign)).wait_recv()

    def b_spread(q, offset):
        piece = wb.at[rows_at(offset, 0)]
        for k in (2, 1, 3):
            n = q * 3 + k - 1
            push(piece, piece, by_send.at[n], by_recv.at[n], at_y(k))

    for load in loads:
        load.wait()
    for k in (2, 1, 3):
        piece = wa.at[own_rows]
        push(piece, piece, ay_send.at[k - 1], ay_recv.at[k - 1], at_y(k))
    z_push(0, 0, 1)
    z_push(0, 1, 1)
    b_spread(0, 0)

    @pl.when(lowest)
    def _():
        pl.semaphore_wait(barrier, 1)

    z_push(1, 0, 1)
    z_push(1, 1, 1)
    bias_load.wait()
    for k in range(1, 8):
        push(bb.at[tp], bb.at[tp], b_send.at[k - 1], b_recv.at[k - 1], at_tp((tp + k) % 8))

    def z_step(p, j):
        for side in (0, 1):
            z_wait(side, p, j)
            if j < 4:
                z_push(side, p, j + 1)
                if p == 0:
                    b_spread(2 * j - 1 + side, -j if side == 0 else j)
        if j == 4 and p == 0:
            b_spread(7, 4)

    for p in (2, 3, 4):
        piece = wa.at[rows_at(0, shifts[p])]
        k = shifts[p]
        remote(piece, piece, ay_send.at[k - 1], ay_recv.at[k - 1], at_y(k)).wait_recv()
        z_push(0, p, 1)
        z_push(1, p, 1)
    for j in range(1, 5):
        for p in range(5):
            z_step(p, j)
        forward_step(j - 1)
    offsets = (0, -1, 1, -2, 2, -3, 3, 4)
    for q in range(8):
        for k in (1, 3, 2):
            n = q * 3 + k - 1
            piece = wb.at[rows_at(offsets[q], k)]
            remote(piece, piece, by_send.at[n], by_recv.at[n], at_y(k)).wait_recv()

    pl.semaphore_signal(hello.at[0], inc=1, device_id=at_tp(otp), device_id_type=MESH)

    @pl.when((zl >= 2) & (zl <= 4))
    def _():
        pl.semaphore_signal(hello.at[1], inc=1, device_id=at_z(3), device_id_type=MESH)

    @pl.when((zl >= 3) & (zl <= 5))
    def _():
        pl.semaphore_signal(hello.at[1], inc=1, device_id=at_z(-3), device_id_type=MESH)

    def project(tokens, s, d, first, count):
        for g, w in enumerate((wa, wb)):
            out = jnp.dot(tokens, w[...], preferred_element_type=jnp.float32).astype(jnp.bfloat16)
            for n in range(len(d)):
                for v in (0, 1):
                    block = out[n * count : (n + 1) * count, v * 128 : (v + 1) * 128]
                    if g == 0:
                        cache_out[v, s, half, d[n], pl.ds(first, count), :] = block
                    else:
                        kv[v, s, d[n], pl.ds(first, count), :] = block

    def o_copy(s, d, v, where):
        n = d * 4 + s * 2 + v
        return remote(
            kv.at[v, s, d], cache_out.at[v, s, where, d], o_send.at[n], o_recv.at[n], at_tp(otp)
        )

    def send_out(s, d):
        for v in (0, 1):
            o_copy(s, d, v, half).start()

    with jax.named_scope("sib"):
        remote(tbuf.at[ds], tbuf.at[ds], s_send.at[CHUNKS], s_recv.at[CHUNKS], at_tp(stp)).wait_recv()

    def early(n, carry):
        s, which = n % 2, n // 2
        d = jnp.where(which == 0, dm, ds)
        project(tbuf[d, pl.ds(pl.multiple_of(s * 128, 128), 128), :], s, (d,), 0, 128)
        send_out(s, d)
        return carry

    lax.fori_loop(0, 4, early, 0)
    for k in range(EARLY):
        s_arrival(k).wait_recv()

    def early_partner(n, carry):
        d = jnp.where(n == 0, dp, dq)
        project(tbuf[d, pl.ds(0, 128), :], 0, (d,), 0, 128)
        send_out(0, d)
        return carry

    lax.fori_loop(0, 2, early_partner, 0)
    forward_step(4)
    forward_step(5)

    q_load.wait()
    off_load.wait()
    for k in range(1, 8):
        src = (tp - k + 8) % 8
        remote(bb.at[src], bb.at[src], b_send.at[k - 1], b_recv.at[k - 1], at_tp(src)).wait_recv()
    row = lax.broadcasted_iota(jnp.int32, (8, 16), 0)
    col = lax.broadcasted_iota(jnp.int32, (8, 16), 1)
    head = jnp.where(row < 2, tp, otp) * 2 + row % 2
    chosen = (col == head) & (row < 4)
    select = jnp.where(chosen, 1.0, 0.0).astype(jnp.bfloat16)
    offset = jnp.sum(
        jnp.where(chosen, jnp.broadcast_to(off_ref[...], (8, 16)), 0.0), axis=1, keepdims=True
    )
    for d in range(8):
        for s in (0, 1):
            picked = jnp.dot(select, bb[d, s], preferred_element_type=jnp.float32)
            bsel[d, s] = picked
            bias_out[s, :, d * 128 : (d + 1) * 128] = picked[0:2].astype(jnp.bfloat16)
    lane = lax.broadcasted_iota(jnp.int32, (8, 128), 1)
    row8 = lax.broadcasted_iota(jnp.int32, (8, 128), 0)
    own_lane = (lane // 64) == (row8 % 2)

    def attend(s):
        score = jnp.zeros((8, 512), jnp.float32)
        for g, t in enumerate((tp, otp)):
            cols = q_ref[:, pl.ds(pl.multiple_of(t * 128, 128), 128)].astype(jnp.float32)
            spread = jnp.broadcast_to(cols[s : s + 1], (8, 128))
            query = jnp.where(own_lane & (row8 // 2 == g), spread, 0.0).astype(jnp.bfloat16)
            keys = cache_out[0, s, half] if g == 0 else kv[0, s]
            score += lax.dot_general(
                query, keys.reshape(512, 128), (((1,), (1,)), ((), ())),
                preferred_element_type=jnp.float32,
            )
        bias = jnp.concatenate([bsel[half * 4 + d, s] for d in range(4)], axis=1)
        logit = score * 0.125 + offset + bias
        tail = jnp.log1p(jnp.exp(-jnp.abs(logit)))
        fading = -(jnp.maximum(logit, 0.0) + tail)
        ls = jnp.minimum(logit, 0.0) - tail
        blocks = [fading[:, d * 128 : (d + 1) * 128] for d in range(4)]
        within = jnp.dot(
            jnp.concatenate(blocks, axis=0), strictly_later(128),
            precision=lax.Precision.HIGHEST, preferred_element_type=jnp.float32,
        )
        carried = jnp.zeros((8, 1), jnp.float32)
        beyond = [None] * 4
        for d in (3, 2, 1, 0):
            beyond[d] = within[d * 8 : d * 8 + 8] + carried
            carried = carried + jnp.sum(blocks[d], axis=1, keepdims=True)
        weight = jnp.exp(ls + jnp.concatenate(beyond, axis=1))
        high = weight.astype(jnp.bfloat16)
        low = (weight - high.astype(jnp.float32)).astype(jnp.bfloat16)
        both = jnp.concatenate([high, low], axis=0)
        sums = jnp.where(own_lane, jnp.broadcast_to(carried, (8, 128)), 0.0)
        for g in (0, 1):
            values = cache_out[1, s, half] if g == 0 else kv[1, s]
            product = jnp.dot(both, values.reshape(512, 128), preferred_element_type=jnp.float32)
            mixture = jnp.where(own_lane, product[0:8] + product[8:16], 0.0)
            r = 2 * g
            part[g, s : s + 1, :] = mixture[r : r + 1] + mixture[r + 1 : r + 2]
            part[g, 2 + s : 3 + s, :] = sums[r : r + 1] + sums[r + 1 : r + 2]

    with jax.named_scope("att0"):
        attend(0)

    def late(k):
        s_arrival(k).wait_recv()
        here = pl.ds(k * rows_of, rows_of)
        both = jnp.concatenate([tbuf[dp, here, :], tbuf[dq, here, :]], axis=0)
        project(both, 1, (dp, dq), (k - EARLY) * rows_of, rows_of)

    for k in range(EARLY, CHUNKS):
        if k >= 6:
            forward_step(k)
        late(k)
    send_out(1, dp)
    send_out(1, dq)
    with jax.named_scope("att1"):
        attend(1)
    pl.semaphore_wait(hello.at[0], 1)

    @pl.when((zl <= 2) | (zl >= 5))
    def _():
        pl.semaphore_wait(hello.at[1], 1)

    mine = y * 2 + half
    firsts = []
    for k in range(1, 4):
        copy = remote(part.at[0], r1.at[mine], f1_send.at[k], f1_recv.at[mine], at_y(k))
        copy.start()
        firsts.append(copy)
    for k in range(0, 4):
        device = (gr, zl * 4 + (y + k) % 4, otp)
        copy = remote(part.at[1], r1.at[mine], f1_send.at[4 + k], f1_recv.at[mine], device)
        copy.start()
        firsts.append(copy)
    own = pltpu.make_async_copy(part.at[0], r1.at[mine], f1_send.at[0])
    own.start()
    own.wait()
    for k in range(1, 4):
        slot = ((y + k) % 4) * 2 + half
        remote(part.at[0], r1.at[slot], f1_send.at[k], f1_recv.at[slot], at_y(k)).wait_recv()
    for k in range(0, 4):
        slot = ((y + k) % 4) * 2 + 1 - half
        remote(part.at[1], r1.at[slot], f1_send.at[4 + k], f1_recv.at[slot], at_tp(otp)).wait_recv()

    def combine(buf):
        total = buf[7][2:4]
        mixed = buf[7][0:2]
        for n in range(6, -1, -1):
            block = buf[n]
            mixed = mixed + block[0:2] * jnp.exp(total)
            total = total + block[2:4]
        return mixed, total

    mixed, total = combine(r1)
    mid[...] = jnp.concatenate([mixed, total], axis=0)
    seconds = []
    for k in range(1, 8):
        device = (gr, ((zl + k) % 8) * 4 + y, tp)
        copy = remote(mid, r2.at[zl], f2_send.at[k], f2_recv.at[zl], device)
        copy.start()
        seconds.append(copy)
    own = pltpu.make_async_copy(mid, r2.at[zl], f2_send.at[0])
    own.start()
    own.wait()
    for k in range(1, 8):
        slot = (zl + k) % 8
        remote(mid, r2.at[slot], f2_send.at[k], f2_recv.at[slot], at_z(1)).wait_recv()
    mixed, total = combine(r2)
    square = mixed * mixed
    first_head = lax.broadcasted_iota(jnp.int32, (2, 128), 1) < 64
    mean_a = jnp.sum(jnp.where(first_head, square, 0.0), axis=1, keepdims=True) * (1.0 / 64)
    mean_b = jnp.sum(jnp.where(first_head, 0.0, square), axis=1, keepdims=True) * (1.0 / 64)
    read_out[...] = mixed * lax.rsqrt(jnp.where(first_head, mean_a, mean_b) + 1e-06)

    for copy in pending + firsts + seconds:
        copy.wait_send()

    def sent(n, carry):
        s, d = n % 2, n // 2
        for v in (0, 1):
            o_copy(s, d, v, half).wait_send()
            o_copy(s, d, v, 1 - half).wait_recv()
        return carry

    lax.fori_loop(0, 8, sent, 0)


def finish(cache_ref, bias_ref, read_ref, key_out, value_out, bias_out, read_out, sem):
    pairs = (
        (cache_ref.at[0], key_out), (cache_ref.at[1], value_out),
        (bias_ref, bias_out), (read_ref, read_out),
    )
    copies = [pltpu.make_async_copy(src, dst, sem.at[n]) for n, (src, dst) in enumerate(pairs)]
    for copy in copies:
        copy.start()
    for copy in copies:
        copy.wait()


def per_device(tokens, key_weight, value_weight, queries, head_offset, key_bias):
    any_space = pl.BlockSpec(memory_space=pl.ANY)
    vmem = pl.BlockSpec(memory_space=pltpu.VMEM)
    dma = pltpu.SemaphoreType.DMA
    held, bias, reading = pl.pallas_call(
        kernel,
        out_shape=(
            pltpu.VMEM((2, 2, 2, 4, 128, 128), jnp.bfloat16),
            pltpu.VMEM((2, 2, 1024), jnp.bfloat16),
            pltpu.VMEM((2, 128), jnp.float32),
        ),
        in_specs=[any_space] * 6,
        out_specs=(vmem, vmem, vmem),
        scratch_shapes=[
            pltpu.VMEM((4, 256, 2048), jnp.bfloat16),
            pltpu.VMEM((2048, 256), jnp.bfloat16),
            pltpu.VMEM((2048, 256), jnp.bfloat16),
            pltpu.VMEM((2, 2, 4, 128, 128), jnp.bfloat16),
            pltpu.VMEM((8, 2, 16, 128), jnp.bfloat16),
            pltpu.VMEM((8, 2, 8, 128), jnp.float32),
            pltpu.VMEM((2, 4, 128), jnp.float32),
            pltpu.VMEM((8, 4, 128), jnp.float32),
            pltpu.VMEM((4, 128), jnp.float32),
            pltpu.VMEM((8, 4, 128), jnp.float32),
            pltpu.VMEM((2, 1024), jnp.bfloat16),
            pltpu.VMEM((1, 16), jnp.float32),
            dma((8,)),
            dma((CHUNKS,)), dma((CHUNKS,)), dma((CHUNKS + 1,)), dma((CHUNKS + 1,)),
            dma((7,)), dma((7,)),
            dma((3,)), dma((3,)), dma((40,)), dma((40,)), dma((24,)), dma((24,)),
            dma((16,)), dma((16,)),
            dma((8,)), dma((8,)), dma((8,)), dma((8,)),
            pltpu.SemaphoreType.REGULAR((2,)),
        ],
        name="prefill",
        compiler_params=pltpu.CompilerParams(
            collective_id=0, has_side_effects=True, vmem_limit_bytes=24 * 1024 * 1024
        ),
    )(*(
        pltpu.with_memory_space_constraint(argument, pltpu.HBM)
        for argument in (
            tokens.reshape(256, 2048),
            key_weight,
            value_weight,
            queries,
            head_offset.reshape(1, 16),
            jnp.transpose(key_bias, (0, 2, 1)),
        )
    ))
    cache = jax.ShapeDtypeStruct((2, 2, 4, 128, 128), jnp.bfloat16)
    keys, values, bias, reading = pl.pallas_call(
        finish,
        out_shape=(
            cache,
            cache,
            jax.ShapeDtypeStruct((2, 2, 1024), jnp.bfloat16),
            jax.ShapeDtypeStruct((2, 128), jnp.float32),
        ),
        in_specs=[vmem] * 3,
        out_specs=(any_space,) * 4,
        scratch_shapes=[dma((4,))],
        name="finish",
        compiler_params=pltpu.CompilerParams(vmem_limit_bytes=1024 * 1024),
    )(*(pltpu.with_memory_space_constraint(part, pltpu.VMEM) for part in (held, bias, reading)))
    return (
        keys.reshape(2, 1024, 128),
        values.reshape(2, 1024, 128),
        jnp.transpose(bias, (0, 2, 1)),
        reading,
    )


def solution(mesh):
    placed = (
        P("gr", ("sp", "tp"), None),
        P("sp", None),
        P("sp", None),
        P("gr", None),
        P(),
        P("gr", ("sp", "tp"), None),
    )
    return jax.shard_map(
        per_device,
        mesh=mesh,
        in_specs=placed,
        out_specs=(P("gr", "sp", "tp"), P("gr", "sp", "tp"), P("gr", "sp", "tp"), P("gr", "tp")),
        check_vma=False,
    )
```

time: 72.6 us -> 59.6 us (0.82)
  the two profiles are of different devices: /device:TPU:6 before, /device:TPU:1 now
where the time goes in v2:
time: 59.6 us; the launch traced here: 59.2 us
  Pallas kernels  58.5 us (98%)
  between operations  0.64 us (1%)
    pallas_call x1, Pallas kernels, per_device(): pl.pallas_call(kernel, out_shape=(pltpu.VMEM((2, 2, 2, 4, 128, 128), jnp....  57.5 us

profile of v2, /device:TPU:1, one launch (start us, length us, event | category | flops | bytes accessed | tf_op | source)
XLA Modules:
  0.0 59.2 jit_solution(12044061484932692453)
XLA Ops:
  0.6 57.5 %prefill.1 = (bf16[2,2,2,4,128,128]{5,4,3,2,1,0:T(8,128)(2,1)S(1)}, bf16[2,2,1024]{2,1,0:T(2,128)(2,1)S(1)}, f32[2,128]{1,0:T(2,128)S(1)}) custom-call(bf16[256,2048]{1,0:T(8,128)(2,1)} %bitcast.6, bf16[64,1024]{1,0:T(8,128)(2,1)} %kw_ref.1, bf16[64,1024]{1,0:T(8,128)(2,1)} %vw_ref.1, bf16[2,1024]{1,0:T(2,128)(2,1)} %q_hbm.1, f32[1,16]{1,0:T(1,128)} %bitcast.8, ...), custom_call_target="tpu_custom_call" | custom-call | tf_op jit(solution)/shard_map/prefill/pallas_call | solution.py:439
  58.2 1.0 %finish.1 = (bf16[2,2,4,128,128]{4,3,2,1,0:T(8,128)(2,1)}, bf16[2,2,4,128,128]{4,3,2,1,0:T(8,128)(2,1)}, bf16[2,2,1024]{2,1,0:T(2,128)(2,1)}, f32[2,128]{1,0:T(2,128)}) custom-call(bf16[2,2,2,4,128,128]{5,4,3,2,1,0:T(8,128)(2,1)S(1)} %get-tuple-element.11.cache_ref, bf16[2,2,1024]{2,1,0:T(2,128)(2,1)S(1)} %get-tuple-element.12.bias_ref, ...), custom_call_target="tpu_custom_call" | custom-call | tf_op jit(solution)/shard_map/finish/pallas_call | solution.py:485

commit v3 on v2

--- a/solution.py
+++ b/solution.py
@@ -22,9 +22,7 @@
     tok_ref, kw_ref, vw_ref, q_hbm, off_hbm, bias_ref,
     cache_out, bias_out, read_out,
     tbuf, wa, wb, kv, bb, bsel, part, r1, mid, r2, q_ref, off_ref,
-    load_sem, t_send, t_recv, s_send, s_recv, b_send, b_recv,
-    ay_send, ay_recv, z_send, z_recv, by_send, by_recv,
-    o_send, o_recv, f1_send, f1_recv, f2_send, f2_recv, hello,
+    load_sem, send, t_recv, s_recv, ay_recv, z_recv, all_recv, hello,
 ):
     gr, sp, tp = lax.axis_index("gr"), lax.axis_index("sp"), lax.axis_index("tp")
     zl, y = sp // 4, sp % 4
@@ -54,31 +52,27 @@
             device_id=device, device_id_type=MESH,
         )
 
-    pending = []
-
-    def push(*args):
-        copy = remote(*args)
-        copy.start()
-        pending.append(copy)
+    to_pair, along_z, along_y, to_other, of_bias, of_read1, of_read2 = range(7)
+
+    def push(src, dst, kind, recv, device):
+        remote(src, dst, send.at[kind], recv, device).start()
 
     tok_load = pltpu.make_async_copy(tok_ref, tbuf.at[dm], load_sem.at[0])
     tok_load.start()
     own_rows = pl.ds(pl.multiple_of(sp * 64, 64), 64)
-    loads = []
     for n, (w_ref, lane) in enumerate(((kw_ref, 0), (vw_ref, 128))):
         for m, (buf, t) in enumerate(((wa, tp), (wb, otp))):
             cols = pl.ds(pl.multiple_of(t * 128, 128), 128)
             load = pltpu.make_async_copy(
                 w_ref.at[:, cols], buf.at[own_rows, pl.ds(lane, 128)],
-                load_sem.at[1 + n * 2 + m],
+                load_sem.at[1],
             )
             load.start()
-            loads.append(load)
-    bias_load = pltpu.make_async_copy(bias_ref, bb.at[tp], load_sem.at[5])
+    bias_load = pltpu.make_async_copy(bias_ref, bb.at[tp], load_sem.at[2])
     bias_load.start()
-    q_load = pltpu.make_async_copy(q_hbm, q_ref, load_sem.at[6])
+    q_load = pltpu.make_async_copy(q_hbm, q_ref, load_sem.at[3])
     q_load.start()
-    off_load = pltpu.make_async_copy(off_hbm, off_ref, load_sem.at[7])
+    off_load = pltpu.make_async_copy(off_hbm, off_ref, load_sem.at[4])
     off_load.start()
 
     barrier = pltpu.get_barrier_semaphore()
@@ -114,32 +108,30 @@
 
     def t_copy(k):
         piece = (dm, pl.ds(k * rows_of, rows_of))
-        return remote(tbuf.at[piece], tbuf.at[piece], t_send.at[k], t_recv.at[k], at_tp(ptp))
+        return remote(tbuf.at[piece], tbuf.at[piece], send.at[to_pair], t_recv.at[k], at_tp(ptp))
 
     def t_arrival(k):
         piece = (dp, pl.ds(k * rows_of, rows_of))
-        return remote(tbuf.at[piece], tbuf.at[piece], t_send.at[k], t_recv.at[k], at_tp(ptp))
+        return remote(tbuf.at[piece], tbuf.at[piece], send.at[to_pair], t_recv.at[k], at_tp(ptp))
+
+    def s_sem(k):
+        return s_recv.at[0 if k < EARLY else 1]
 
     def t_forward(k):
         piece = (dp, pl.ds(k * rows_of, rows_of))
-        return remote(tbuf.at[piece], tbuf.at[piece], s_send.at[k], s_recv.at[k], at_tp(stp))
-
-    def s_arrival(k):
-        piece = (dq, pl.ds(k * rows_of, rows_of))
-        return remote(tbuf.at[piece], tbuf.at[piece], s_send.at[k], s_recv.at[k], at_tp(stp))
+        return remote(tbuf.at[piece], tbuf.at[piece], send.at[to_pair], s_sem(k), at_tp(stp))
 
     def forward_step(k):
         t_arrival(k).wait_recv()
-        copy = t_forward(k)
-        copy.start()
-        pending.append(copy)
-
+        t_forward(k).start()
+
+    bias_load.wait()
+    for k in range(1, 8):
+        push(bb.at[tp], bb.at[tp], of_bias, all_recv.at[0], at_tp((tp + k) % 8))
     tok_load.wait()
     for k in range(CHUNKS):
-        copy = t_copy(k)
-        copy.start()
-        pending.append(copy)
-    push(tbuf.at[dm], tbuf.at[dm], s_send.at[CHUNKS], s_recv.at[CHUNKS], at_tp(stp))
+        t_copy(k).start()
+    push(tbuf.at[dm], tbuf.at[dm], to_pair, s_recv.at[2], at_tp(stp))
 
     shifts = (0, 0, 1, 3, 2)
 
@@ -157,38 +149,34 @@
         else:
             piece = z_piece(p, -sign * 3, 32 * side, 32)
         n = (side * 5 + p) * 4 + j - 1
-        push(piece, piece, z_send.at[n], z_recv.at[n], at_z(sign))
+        push(piece, piece, along_z, z_recv.at[n], at_z(sign))
 
     def z_wait(side, p, j):
         sign = 1 if side == 0 else -1
         piece = z_piece(p, -sign * j) if j < 4 else z_piece(p, 4, 32 * side, 32)
         n = (side * 5 + p) * 4 + j - 1
-        remote(piece, piece, z_send.at[n], z_recv.at[n], at_z(sign)).wait_recv()
-
-    def b_spread(q, offset):
+        remote(piece, piece, send.at[along_z], z_recv.at[n], at_z(sign)).wait_recv()
+
+    def b_spread(offset):
         piece = wb.at[rows_at(offset, 0)]
         for k in (2, 1, 3):
-            n = q * 3 + k - 1
-            push(piece, piece, by_send.at[n], by_recv.at[n], at_y(k))
-
-    for load in loads:
-        load.wait()
+            push(piece, piece, along_y, all_recv.at[1], at_y(k))
+
+    pltpu.make_async_copy(kw_ref.at[:, 0:512], kw_ref.at[:, 0:512], load_sem.at[1]).wait()
     for k in (2, 1, 3):
         piece = wa.at[own_rows]
-        push(piece, piece, ay_send.at[k - 1], ay_recv.at[k - 1], at_y(k))
+        push(piece, piece, along_y, ay_recv.at[k - 1], at_y(k))
+    b_spread(0)
+
+    @pl.when(lowest)
+    def _():
+        pl.semaphore_wait(barrier, 1)
+
     z_push(0, 0, 1)
     z_push(0, 1, 1)
-    b_spread(0, 0)
-
-    @pl.when(lowest)
-    def _():
-        pl.semaphore_wait(barrier, 1)
 
     z_push(1, 0, 1)
     z_push(1, 1, 1)
-    bias_load.wait()
-    for k in range(1, 8):
-        push(bb.at[tp], bb.at[tp], b_send.at[k - 1], b_recv.at[k - 1], at_tp((tp + k) % 8))
 
     def z_step(p, j):
         for side in (0, 1):
@@ -196,26 +184,28 @@
             if j < 4:
                 z_push(side, p, j + 1)
                 if p == 0:
-                    b_spread(2 * j - 1 + side, -j if side == 0 else j)
+                    b_spread(-j if side == 0 else j)
         if j == 4 and p == 0:
-            b_spread(7, 4)
-
+            b_spread(4)
+
+    z_step(0, 1)
     for p in (2, 3, 4):
         piece = wa.at[rows_at(0, shifts[p])]
         k = shifts[p]
-        remote(piece, piece, ay_send.at[k - 1], ay_recv.at[k - 1], at_y(k)).wait_recv()
+        remote(piece, piece, send.at[along_y], ay_recv.at[k - 1], at_y(k)).wait_recv()
         z_push(0, p, 1)
         z_push(1, p, 1)
-    for j in range(1, 5):
+        if p == 2:
+            z_step(1, 1)
+    for p in (2, 3, 4):
+        z_step(p, 1)
+    forward_step(0)
+    for j in range(2, 5):
         for p in range(5):
             z_step(p, j)
         forward_step(j - 1)
-    offsets = (0, -1, 1, -2, 2, -3, 3, 4)
-    for q in range(8):
-        for k in (1, 3, 2):
-            n = q * 3 + k - 1
-            piece = wb.at[rows_at(offsets[q], k)]
-            remote(piece, piece, by_send.at[n], by_recv.at[n], at_y(k)).wait_recv()
+    piece = wb.at[pl.ds(0, 24 * 64)]
+    remote(piece, piece, send.at[along_y], all_recv.at[1], at_y(1)).wait_recv()
 
     pl.semaphore_signal(hello.at[0], inc=1, device_id=at_tp(otp), device_id_type=MESH)
 
@@ -238,18 +228,14 @@
                     else:
                         kv[v, s, d[n], pl.ds(first, count), :] = block
 
-    def o_copy(s, d, v, where):
-        n = d * 4 + s * 2 + v
-        return remote(
-            kv.at[v, s, d], cache_out.at[v, s, where, d], o_send.at[n], o_recv.at[n], at_tp(otp)
-        )
-
     def send_out(s, d):
         for v in (0, 1):
-            o_copy(s, d, v, half).start()
-
-    with jax.named_scope("sib"):
-        remote(tbuf.at[ds], tbuf.at[ds], s_send.at[CHUNKS], s_recv.at[CHUNKS], at_tp(stp)).wait_recv()
+            push(kv.at[v, s, d], cache_out.at[v, s, half, d], to_other, all_recv.at[2], at_tp(otp))
+
+    remote(tbuf.at[ds], tbuf.at[ds], send.at[to_pair], s_recv.at[2], at_tp(stp)).wait_recv()
+
+    for k in range(EARLY, CHUNKS - 1):
+        forward_step(k)
 
     def early(n, carry):
         s, which = n % 2, n // 2
@@ -259,24 +245,21 @@
         return carry
 
     lax.fori_loop(0, 4, early, 0)
-    for k in range(EARLY):
-        s_arrival(k).wait_recv()
+    piece = (dq, pl.ds(0, EARLY * rows_of))
+    remote(tbuf.at[piece], tbuf.at[piece], send.at[to_pair], s_sem(0), at_tp(stp)).wait_recv()
 
     def early_partner(n, carry):
         d = jnp.where(n == 0, dp, dq)
         project(tbuf[d, pl.ds(0, 128), :], 0, (d,), 0, 128)
-        send_out(0, d)
         return carry
 
     lax.fori_loop(0, 2, early_partner, 0)
-    forward_step(4)
-    forward_step(5)
+    forward_step(CHUNKS - 1)
 
     q_load.wait()
     off_load.wait()
-    for k in range(1, 8):
-        src = (tp - k + 8) % 8
-        remote(bb.at[src], bb.at[src], b_send.at[k - 1], b_recv.at[k - 1], at_tp(src)).wait_recv()
+    piece = bb.at[pl.ds(0, 7)]
+    remote(piece, piece, send.at[of_bias], all_recv.at[0], at_tp(otp)).wait_recv()
     row = lax.broadcasted_iota(jnp.int32, (8, 16), 0)
     col = lax.broadcasted_iota(jnp.int32, (8, 16), 1)
     head = jnp.where(row < 2, tp, otp) * 2 + row % 2
@@ -333,23 +316,18 @@
             part[g, s : s + 1, :] = mixture[r : r + 1] + mixture[r + 1 : r + 2]
             part[g, 2 + s : 3 + s, :] = sums[r : r + 1] + sums[r + 1 : r + 2]
 
-    with jax.named_scope("att0"):
-        attend(0)
-
-    def late(k):
-        s_arrival(k).wait_recv()
-        here = pl.ds(k * rows_of, rows_of)
-        both = jnp.concatenate([tbuf[dp, here, :], tbuf[dq, here, :]], axis=0)
-        project(both, 1, (dp, dq), (k - EARLY) * rows_of, rows_of)
-
-    for k in range(EARLY, CHUNKS):
-        if k >= 6:
-            forward_step(k)
-        late(k)
-    send_out(1, dp)
-    send_out(1, dq)
-    with jax.named_scope("att1"):
-        attend(1)
+    attend(0)
+
+    piece = (dq, pl.ds(EARLY * rows_of, 128))
+    remote(tbuf.at[piece], tbuf.at[piece], send.at[to_pair], s_recv.at[1], at_tp(stp)).wait_recv()
+
+    def late(n, carry):
+        d = jnp.where(n == 0, dp, dq)
+        project(tbuf[d, pl.ds(128, 128), :], 1, (d,), 0, 128)
+        return carry
+
+    lax.fori_loop(0, 2, late, 0)
+    attend(1)
     pl.semaphore_wait(hello.at[0], 1)
 
     @pl.when((zl <= 2) | (zl >= 5))
@@ -357,25 +335,16 @@
         pl.semaphore_wait(hello.at[1], 1)
 
     mine = y * 2 + half
-    firsts = []
-    for k in range(1, 4):
-        copy = remote(part.at[0], r1.at[mine], f1_send.at[k], f1_recv.at[mine], at_y(k))
-        copy.start()
-        firsts.append(copy)
-    for k in range(0, 4):
-        device = (gr, zl * 4 + (y + k) % 4, otp)
-        copy = remote(part.at[1], r1.at[mine], f1_send.at[4 + k], f1_recv.at[mine], device)
-        copy.start()
-        firsts.append(copy)
-    own = pltpu.make_async_copy(part.at[0], r1.at[mine], f1_send.at[0])
-    own.start()
-    own.wait()
-    for k in range(1, 4):
-        slot = ((y + k) % 4) * 2 + half
-        remote(part.at[0], r1.at[slot], f1_send.at[k], f1_recv.at[slot], at_y(k)).wait_recv()
-    for k in range(0, 4):
-        slot = ((y + k) % 4) * 2 + 1 - half
-        remote(part.at[1], r1.at[slot], f1_send.at[4 + k], f1_recv.at[slot], at_tp(otp)).wait_recv()
+    for k in (2, 1, 3):
+        push(part.at[1], r1.at[mine], of_read1, all_recv.at[3], (gr, zl * 4 + (y + k) % 4, otp))
+        push(part.at[0], r1.at[mine], of_read1, all_recv.at[3], at_y(k))
+    push(part.at[1], r1.at[mine], of_read1, all_recv.at[3], at_tp(otp))
+    r1[mine] = part[0]
+    for s in (0, 1):
+        send_out(s, dp)
+        send_out(s, dq)
+    piece = r1.at[pl.ds(0, 7)]
+    remote(piece, piece, send.at[of_read1], all_recv.at[3], at_tp(otp)).wait_recv()
 
     def combine(buf):
         total = buf[7][2:4]
@@ -388,18 +357,11 @@
 
     mixed, total = combine(r1)
     mid[...] = jnp.concatenate([mixed, total], axis=0)
-    seconds = []
-    for k in range(1, 8):
-        device = (gr, ((zl + k) % 8) * 4 + y, tp)
-        copy = remote(mid, r2.at[zl], f2_send.at[k], f2_recv.at[zl], device)
-        copy.start()
-        seconds.append(copy)
-    own = pltpu.make_async_copy(mid, r2.at[zl], f2_send.at[0])
-    own.start()
-    own.wait()
-    for k in range(1, 8):
-        slot = (zl + k) % 8
-        remote(mid, r2.at[slot], f2_send.at[k], f2_recv.at[slot], at_z(1)).wait_recv()
+    r2[zl] = jnp.concatenate([mixed, total], axis=0)
+    for k in range(7, 0, -1):
+        push(mid, r2.at[zl], of_read2, all_recv.at[4], (gr, ((zl + k) % 8) * 4 + y, tp))
+    piece = r2.at[pl.ds(0, 7)]
+    remote(piece, piece, send.at[of_read2], all_recv.at[4], at_z(1)).wait_recv()
     mixed, total = combine(r2)
     square = mixed * mixed
     first_head = lax.broadcasted_iota(jnp.int32, (2, 128), 1) < 64
@@ -407,17 +369,17 @@
     mean_b = jnp.sum(jnp.where(first_head, 0.0, square), axis=1, keepdims=True) * (1.0 / 64)
     read_out[...] = mixed * lax.rsqrt(jnp.where(first_head, mean_a, mean_b) + 1e-06)
 
-    for copy in pending + firsts + seconds:
-        copy.wait_send()
-
-    def sent(n, carry):
-        s, d = n % 2, n // 2
-        for v in (0, 1):
-            o_copy(s, d, v, half).wait_send()
-            o_copy(s, d, v, 1 - half).wait_recv()
-        return carry
-
-    lax.fori_loop(0, 8, sent, 0)
+    remote(kv, kv, send.at[to_other], all_recv.at[2], at_tp(otp)).wait_recv()
+    for kind, whole in (
+        (to_pair, tbuf.at[pl.ds(0, 3)]),
+        (along_z, tbuf.at[:, pl.ds(0, 224), pl.ds(0, 640)]),
+        (along_y, tbuf.at[:, pl.ds(0, 144), pl.ds(0, 768)]),
+        (to_other, kv),
+        (of_bias, bb.at[pl.ds(0, 7)]),
+        (of_read1, r1.at[pl.ds(0, 7)]),
+        (of_read2, r2.at[pl.ds(0, 7)]),
+    ):
+        remote(whole, whole, send.at[kind], all_recv.at[0], at_tp(otp)).wait_send()
 
 
 def finish(cache_ref, bias_ref, read_ref, key_out, value_out, bias_out, read_out, sem):
@@ -458,12 +420,8 @@
             pltpu.VMEM((8, 4, 128), jnp.float32),
             pltpu.VMEM((2, 1024), jnp.bfloat16),
             pltpu.VMEM((1, 16), jnp.float32),
-            dma((8,)),
-            dma((CHUNKS,)), dma((CHUNKS,)), dma((CHUNKS + 1,)), dma((CHUNKS + 1,)),
-            dma((7,)), dma((7,)),
-            dma((3,)), dma((3,)), dma((40,)), dma((40,)), dma((24,)), dma((24,)),
-            dma((16,)), dma((16,)),
-            dma((8,)), dma((8,)), dma((8,)), dma((8,)),
+            dma((5,)), dma((7,)),
+            dma((CHUNKS,)), dma((3,)), dma((3,)), dma((40,)), dma((5,)),
             pltpu.SemaphoreType.REGULAR((2,)),
         ],
         name="prefill",

time: 59.6 us -> 54.2 us (0.909)
  Pallas kernels: 58.5 us -> 53.4 us
    pallas_call x1, Pallas kernels: 57.5 us -> 52.4 us  [per_device(): pl.pallas_call(kernel, out_shape=(pltpu.VMEM((2, 2, 2, 4, 128, 128), jnp....]
where the time goes in v3:
time: 54.2 us; the launch traced here: 54.1 us
  Pallas kernels  53.4 us (99%)
  between operations  0.64 us (1%)
    pallas_call x1, Pallas kernels, per_device(): pl.pallas_call(kernel, out_shape=(pltpu.VMEM((2, 2, 2, 4, 128, 128), jnp....  52.4 us

profile of v3, /device:TPU:1, one launch (start us, length us, event | category | flops | bytes accessed | tf_op | source)
XLA Modules:
  0.0 54.1 jit_solution(1862258865353547655)
XLA Ops:
  0.6 52.4 %prefill.1 = (bf16[2,2,2,4,128,128]{5,4,3,2,1,0:T(8,128)(2,1)S(1)}, bf16[2,2,1024]{2,1,0:T(2,128)(2,1)S(1)}, f32[2,128]{1,0:T(2,128)S(1)}) custom-call(bf16[256,2048]{1,0:T(8,128)(2,1)} %bitcast.6, bf16[64,1024]{1,0:T(8,128)(2,1)} %kw_ref.1, bf16[64,1024]{1,0:T(8,128)(2,1)} %vw_ref.1, bf16[2,1024]{1,0:T(2,128)(2,1)} %q_hbm.1, f32[1,16]{1,0:T(1,128)} %bitcast.8, ...), custom_call_target="tpu_custom_call" | custom-call | tf_op jit(solution)/shard_map/prefill/pallas_call | solution.py:401
  53.1 1.0 %finish.1 = (bf16[2,2,4,128,128]{4,3,2,1,0:T(8,128)(2,1)}, bf16[2,2,4,128,128]{4,3,2,1,0:T(8,128)(2,1)}, bf16[2,2,1024]{2,1,0:T(2,128)(2,1)}, f32[2,128]{1,0:T(2,128)}) custom-call(bf16[2,2,2,4,128,128]{5,4,3,2,1,0:T(8,128)(2,1)S(1)} %get-tuple-element.11.cache_ref, bf16[2,2,1024]{2,1,0:T(2,128)(2,1)S(1)} %get-tuple-element.12.bias_ref, ...), custom_call_target="tpu_custom_call" | custom-call | tf_op jit(solution)/shard_map/finish/pallas_call | solution.py:443
